TPU v7x, 32 devices: a whole 2x2x4 slice. The times are simulated.
32 devices in a mesh: sp: 8 (over z, y), tp: 4 (over x, core).
Axes of the slice: x: 2, y: 2, z: 4, core: 2. Of those that a mesh axis runs over, the one named last changes fastest.
Arguments:
- conv_input: bfloat16 [4096, 1024], P('sp', 'tp'), may hold values from -6 to 6
- gate_inner: bfloat16 [4096, 1024], P('sp', 'tp'), may hold values from -6 to 6
- gate_outer: bfloat16 [4096, 1024], P('sp', 'tp'), may hold values from -6 to 6
- conv_taps: bfloat16 [3, 1024], P(None, 'tp'), may hold values from -3.5 to 3.5
- doc_ids: int32 [4096], P('sp'), may hold values from 0 to 3, never falling along the last dimension, each value on 1 to 2048 neighbouring positions
- residual_in: bfloat16 [4096, 2048], P(('sp', 'tp')), may hold values from -6 to 6
- out_proj: bfloat16 [1024, 2048], replicated, may hold values from -0.1875 to 0.1875
- norm_gain: float32 [2048], replicated, may hold values from 0.1 to 1.9
- expert_ids: int32 [4096, 2], P(('sp', 'tp')), may hold values from 0 to 31, all different within a row; in each aligned block of 128 rows (0 to 127, 128 to 255, ...) at most 16 rows name the same one
- expert_weights: float32 [4096, 2], P(('sp', 'tp')), may hold values from 0.2 to 1
- gate_proj: bfloat16 [32, 2048, 1024], P(('sp', 'tp')), may hold values from -0.125 to 0.125
- up_proj: bfloat16 [32, 2048, 1024], P(('sp', 'tp')), may hold values from -0.125 to 0.125
- down_proj: bfloat16 [32, 1024, 2048], P(('sp', 'tp')), may hold values from -0.1875 to 0.1875
Outputs:
- layer_out: bfloat16 [4096, 2048], P(('sp', 'tp'))
Inputs may be any that keep to these rules, and one draw needn't show every extreme that they name: `doc_ids`: never falls along positions; each document has at most 2048 positions. `expert_ids`: each row names 2 different experts; within the rows of one device, aligned blocks of 128 rows, no expert is named more than 16 times, a bound that some block reaches.
All inputs are finite; a program needn't handle non-finite values.
Results may differ from a plain program's by a relative error of at most 0.009.
Values may be sent and summed in bfloat16 or wider, within the bound.
A program may use at most 64 MiB of HBM per device.

v0:
```python
import jax
import jax.numpy as jnp
from jax import lax
from jax.sharding import PartitionSpec as P


def from_behind(block, axis, distance):
    devices = range(lax.axis_size(axis))
    route = [(i - distance, i) for i in devices if i - distance in devices]
    return lax.ppermute(block, axis, route)


def expert_rows(arrived, gate_weight, up_weight, down_weight):
    gate_value = jnp.dot(arrived, gate_weight, preferred_element_type=jnp.float32)
    up_value = jnp.dot(arrived, up_weight, preferred_element_type=jnp.float32)
    hidden = (jax.nn.silu(gate_value) * up_value).astype(jnp.bfloat16)
    return jnp.dot(hidden, down_weight, preferred_element_type=jnp.float32).astype(jnp.bfloat16)


def on_device(
    conv_input,
    gate_inner,
    gate_outer,
    conv_taps,
    doc_ids,
    residual_in,
    out_proj,
    norm_gain,
    expert_ids,
    expert_weights,
    gate_proj,
    up_proj,
    down_proj,
):
    inner_prod = conv_input.astype(jnp.float32) * gate_inner.astype(jnp.float32)
    earlier, earlier_docs = from_behind((inner_prod[-2:], doc_ids[-2:]), "sp", 1)
    padded = jnp.concatenate([earlier, inner_prod], axis=0)
    padded_docs = jnp.concatenate([earlier_docs, doc_ids], axis=0)
    length = inner_prod.shape[0]
    tap_values = conv_taps.astype(jnp.float32)
    one_back = jnp.where(
        (padded_docs[1 : length + 1] == doc_ids)[:, None], padded[1 : length + 1], 0.0
    )
    two_back = jnp.where((padded_docs[:length] == doc_ids)[:, None], padded[:length], 0.0)
    mixed_rows = tap_values[2] * inner_prod + tap_values[1] * one_back + tap_values[0] * two_back
    conv_out = (gate_outer.astype(jnp.float32) * mixed_rows).astype(jnp.bfloat16)
    row_count = residual_in.shape[0]
    regrouped = lax.all_to_all(conv_out, "tp", split_axis=0, concat_axis=1, tiled=True)
    mix = jnp.dot(regrouped, out_proj, preferred_element_type=jnp.float32).astype(jnp.bfloat16)
    carried = residual_in.astype(jnp.float32) + mix.astype(jnp.float32)
    normed = (
        carried * lax.rsqrt(jnp.mean(carried * carried, axis=1, keepdims=True) + 1e-06) * norm_gain
    ).astype(jnp.bfloat16)
    model_width = normed.shape[1]
    choose = expert_ids.shape[1]
    sp_count = lax.axis_size("sp")
    tp_count = lax.axis_size("tp")
    experts_total = sp_count * tp_count
    capacity = 2 * row_count * choose // experts_total
    flat_ids = expert_ids.reshape(-1)
    onehot = (flat_ids[:, None] == jnp.arange(experts_total, dtype=jnp.int32)[None, :]).astype(
        jnp.int32
    )
    slot_rank = jnp.sum((jnp.cumsum(onehot, axis=0) - 1) * onehot, axis=1)
    target = flat_ids * capacity + slot_rank
    sources = jnp.repeat(normed, choose, axis=0)
    outgoing = (
        jnp.zeros((experts_total * capacity, model_width), jnp.bfloat16).at[target].set(sources)
    )
    gate_weight = gate_proj[0]
    up_weight = up_proj[0]
    down_weight = down_proj[0]
    arrived = lax.all_to_all(
        outgoing.reshape(experts_total, capacity, model_width),
        ("sp", "tp"),
        split_axis=0,
        concat_axis=0,
        tiled=True,
    )
    item_count = arrived.shape[1]
    flat_rows = arrived.reshape(-1, model_width)
    result = expert_rows(flat_rows, gate_weight, up_weight, down_weight)
    result = result.reshape(experts_total, item_count, model_width)
    returned = lax.all_to_all(result, ("sp", "tp"), split_axis=0, concat_axis=0, tiled=True)
    picked = (
        returned.reshape(-1, model_width)[target]
        .reshape(row_count, choose, model_width)
        .astype(jnp.float32)
    )
    combined = carried + jnp.sum(expert_weights[:, :, None] * picked, axis=1)
    return combined.astype(jnp.bfloat16)


def solution(mesh):
    in_specs = (
        P("sp", "tp"),
        P("sp", "tp"),
        P("sp", "tp"),
        P(None, "tp"),
        P("sp"),
        P(("sp", "tp"), None),
        P(),
        P(),
        P(("sp", "tp"), None),
        P(("sp", "tp"), None),
        P(("sp", "tp"), None, None),
        P(("sp", "tp"), None, None),
        P(("sp", "tp"), None, None),
    )
    out_specs = P(("sp", "tp"), None)
    return jax.shard_map(
        on_device, mesh=mesh, in_specs=in_specs, out_specs=out_specs, check_vma=False
    )
```

profile of v0, /device:TPU:0, one launch (start us, length us, event | category | flops | bytes accessed | tf_op | source)
XLA Modules:
  0.0 163.1 jit_solution(4871068984144054818)
XLA Ops:
  0.0 1.1 convert_multiply_fusion
  1.2 4.9 %collective-permute-start.1 = (f32[2,256]{1,0:T(2,128)S(1)}, f32[2,256]{1,0:T(2,128)S(1)}, u32[]{:S(2)}, u32[]{:S(2)}) collective-permute-start(f32[2,256]{1,0:T(2,128)S(1)} %slice.48), channel_id=1, source_target_pairs={{0,4},{4,8},{8,12},{12,16},{16,20},{20,24},{24,28},{1,5},{5,9},{9,... | collective-permute-start | bytes 6152 | tf_op jit(solution)/shard_map/ppermute | solution.py:10
  6.1 0.8 slice.35
  6.8 3.4 %collective-permute-start = (s32[2]{0:T(128)S(1)}, s32[2]{0:T(128)S(1)}, u32[]{:S(2)}, u32[]{:S(2)}) collective-permute-start(s32[2]{0:T(128)S(1)} %slice.35), channel_id=1, source_target_pairs={{0,4},{4,8},{8,12},{12,16},{16,20},{20,24},{24,28},{1,5},{5,9},{9,... | collective-permute-start | bytes 32 | tf_op jit(solution)/shard_map/ppermute | solution.py:10
  10.2 0.8 copy.23
  12.0 0.8 fusion.30
  14.0 0.8 pad_add_fusion
  14.8 0.8 slice_compare_fusion.1
  15.5 1.9 %fusion.23 = bf16[512,256]{1,0:T(8,128)(2,1)} fusion(f32[2,256]{1,0:T(2,128)S(1)} %collective-permute-done.1, f32[512,256]{1,0:T(8,128)S(1)} %convert_multiply_fusion, bf16[512,256]{1,0:T(8,128)(2,1)} %param.15, f32[256]{0:T(256)S(1)} %bitcast.58, f32[256]{0:T(256)S(1)} %bitcast.57, f32[256]{0:T(256)S(1)} %bitcast.56, ...), kind=kLoop, calls=%fused_computation.27 | loop fusion | flops 1572864 | bytes 1054720 | tf_op jit(solution)/shard_map/convert_element_type | solution.py:46
  17.5 3.4 %all-to-all-start = ((bf16[4,128,256]{2,1,0:T(8,128)(2,1)}), bf16[4,128,256]{2,1,0:T(8,128)(2,1)S(1)}, u32[]{:S(2)}, u32[]{:S(2)}) async-start(bf16[4,128,256]{2,1,0:T(8,128)(2,1)} %bitcast.3), calls=%async_computation | async-start | bytes 524288 | tf_op jit(solution)/shard_map/all_to_all | solution.py:48
  20.9 6.0 %all-to-all-done = bf16[4,128,256]{2,1,0:T(8,128)(2,1)S(1)} async-done(((bf16[4,128,256]{2,1,0:T(8,128)(2,1)}), bf16[4,128,256]{2,1,0:T(8,128)(2,1)S(1)}, u32[]{:S(2)}, u32[]{:S(2)}) %all-to-all-start) | async-done | bytes 262176 | tf_op jit(solution)/shard_map/all_to_all | solution.py:48
  27.0 3.0 %multiply_reduce_fusion.1 = (f32[128]{0:T(128)S(1)}, f32[128,2048]{1,0:T(8,128)S(1)}) fusion(bf16[128,1024]{0,1:T(8,128)(2,1)S(1)} %bitcast.51, bf16[1024,2048]{1,0:T(8,128)(2,1)} %param.19, bf16[128,2048]{1,0:T(8,128)(2,1)S(1)} %copy-done.1), kind=kOutput, calls=%fused_computation.16 | convolution fusion | flops 538443648 | bytes 6029824 | tf_op jit(solution)/shard_map/dot_general | solution.py:49
  30.9 1.2 reshape.100
  32.1 3.5 %scatter_custom_fusion = bf16[512,2048]{1,0:T(8,128)(2,1)S(1)} fusion(s32[256]{0:T(256)S(1)} %bitcast.53, bf16[256,2048]{1,0:T(8,128)(2,1)} %reshape.100, bf16[]{:T(256)} %constant.6.clone.1), kind=kCustom, calls=%fused_computation.17 | custom fusion | bytes 2097664 | tf_op jit(solution)/shard_map/scatter | solution.py:68
  35.6 52.4 %all_to_all.29 = bf16[32,16,2048]{2,1,0:T(8,128)(2,1)S(1)} all-to-all(bf16[32,16,2048]{2,1,0:T(8,128)(2,1)S(1)} %bitcast.47), channel_id=1, replica_groups=mesh['sp'=8,'tp'=4] {'sp','tp'}, dimensions={0} | all-to-all | bytes 4194304 | tf_op jit(solution)/shard_map/all_to_all | solution.py:73
  88.0 1.3 copy-done
  89.4 2.3 %fusion.4 = f32[512,1024]{1,0:T(8,128)S(1)} fusion(bf16[512,2048]{1,0:T(8,128)(2,1)S(1)} %bitcast.49, bf16[1,2048,1024]{2,1,0:T(8,128)(2,1)S(1)} %copy-done.4), kind=kOutput, calls=%fused_computation.6 | convolution fusion | flops 2147483648 | bytes 8388608 | tf_op jit(solution)/shard_map/dot_general | solution.py:14
  91.7 9.9 %fusion.6 = bf16[512,2048]{1,0:T(8,128)(2,1)} fusion(bf16[1,1024,2048]{2,1,0:T(8,128)(2,1)} %param.25, f32[512,1024]{1,0:T(8,128)S(1)} %fusion.4, bf16[512,2048]{1,0:T(8,128)(2,1)} %bitcast.50, bf16[1,2048,1024]{2,1,0:T(8,128)(2,1)} %param.24), kind=kOutput, calls=%fused_computation.8 | convolution fusion | flops 4299161600 | bytes 14680064 | tf_op jit(solution)/shard_map/dot_general | solution.py:17
  101.7 3.8 %all-to-all-start.2 = ((bf16[32,16,2048]{2,1,0:T(8,128)(2,1)}), bf16[32,16,2048]{2,1,0:T(8,128)(2,1)S(1)}, u32[]{:S(2)}, u32[]{:S(2)}) async-start(bf16[32,16,2048]{2,1,0:T(8,128)(2,1)} %bitcast.48), calls=%async_computation.2 | async-start | bytes 4194304 | tf_op jit(solution)/shard_map/all_to_all | solution.py:84
  105.7 48.5 %all-to-all-done.2 = bf16[32,16,2048]{2,1,0:T(8,128)(2,1)S(1)} async-done(((bf16[32,16,2048]{2,1,0:T(8,128)(2,1)}), bf16[32,16,2048]{2,1,0:T(8,128)(2,1)S(1)}, u32[]{:S(2)}, u32[]{:S(2)}) %all-to-all-start.2) | async-done | bytes 2097184 | tf_op jit(solution)/shard_map/all_to_all | solution.py:84
  154.2 2.3 %gather_fusion = bf16[256,2048]{1,0:T(8,128)(2,1)} fusion(bf16[512,2048]{1,0:T(8,128)(2,1)S(1)} %bitcast.46, s32[1024]{0:T(1024)S(1)} %pad_clamp_fusion), kind=kCustom, calls=%fused_computation | custom fusion | bytes 2098176 | tf_op jit(solution)/shard_map/gather | solution.py:86
  156.6 2.4 %reshape.87 = f32[128,2,2048]{2,1,0:T(2,128)S(1)} reshape(bf16[256,2048]{1,0:T(8,128)(2,1)} %gather_fusion) | data formatting | bytes 3145728 | tf_op jit(solution)/shard_map/convert_element_type | solution.py:88
  158.9 3.2 %multiply_reduce_fusion = f32[128,2048]{1,0:T(8,128)S(1)} fusion(f32[128,2,2048]{2,1,0:T(2,128)S(1)} %reshape.87, f32[128,2]{1,0:T(8,128)S(1)} %copy.21), kind=kLoop, calls=%fused_computation.12 | loop fusion | flops 786432 | bytes 3146752 | tf_op jit(solution)/shard_map/reduce_sum | solution.py:90
  162.1 0.9 add_convert_fusion
  (30 shorter events, 3.3 us)
Async XLA Ops:
  0.0 27.0 %copy-start.1 = (bf16[128,2048]{1,0:T(8,128)(2,1)S(1)}, bf16[128,2048]{1,0:T(8,128)(2,1)}, u32[]{:S(2)}) copy-start(bf16[128,2048]{1,0:T(8,128)(2,1)} %param.18) | copy-start | bytes 1572868
  1.2 14.4 %collective-permute-start.1 = (f32[2,256]{1,0:T(2,128)S(1)}, f32[2,256]{1,0:T(2,128)S(1)}, u32[]{:S(2)}, u32[]{:S(2)}) collective-permute-start(f32[2,256]{1,0:T(2,128)S(1)} %slice.48), channel_id=1, source_target_pairs={{0,4},{4,8},{8,12},{12,16},{16,20},{20,24},{24,28},{1,5},{5,9},{9,... | collective-permute-start | bytes 6152 | tf_op jit(solution)/shard_map/ppermute | solution.py:10
  6.8 7.2 %collective-permute-start = (s32[2]{0:T(128)S(1)}, s32[2]{0:T(128)S(1)}, u32[]{:S(2)}, u32[]{:S(2)}) collective-permute-start(s32[2]{0:T(128)S(1)} %slice.35), channel_id=1, source_target_pairs={{0,4},{4,8},{8,12},{12,16},{16,20},{20,24},{24,28},{1,5},{5,9},{9,... | collective-permute-start | bytes 32 | tf_op jit(solution)/shard_map/ppermute | solution.py:10
  17.5 9.4 %all-to-all-start = ((bf16[4,128,256]{2,1,0:T(8,128)(2,1)}), bf16[4,128,256]{2,1,0:T(8,128)(2,1)S(1)}, u32[]{:S(2)}, u32[]{:S(2)}) async-start(bf16[4,128,256]{2,1,0:T(8,128)(2,1)} %bitcast.3), calls=%async_computation | async-start | bytes 524288 | tf_op jit(solution)/shard_map/all_to_all | solution.py:48
  27.0 3.0 %copy-start.2 = (f32[2048]{0:T(1024)S(1)}, f32[2048]{0:T(1024)}, u32[]{:S(2)}) copy-start(f32[2048]{0:T(1024)} %param.20) | copy-start | bytes 24580
  35.6 53.8 %copy-start.4 = (bf16[1,2048,1024]{2,1,0:T(8,128)(2,1)S(1)}, bf16[1,2048,1024]{2,1,0:T(8,128)(2,1)}, u32[]{:S(2)}) copy-start(bf16[1,2048,1024]{2,1,0:T(8,128)(2,1)} %param.23) | copy-start | bytes 12582916
  88.0 1.4 copy-start
  101.7 3.9 %copy-start.3 = (f32[128,2]{0,1:T(2,128)S(1)}, f32[128,2]{0,1:T(2,128)}, u32[]{:S(2)}) copy-start(f32[128,2]{0,1:T(2,128)} %param.22) | copy-start | bytes 3076
  101.7 52.5 %all-to-all-start.2 = ((bf16[32,16,2048]{2,1,0:T(8,128)(2,1)}), bf16[32,16,2048]{2,1,0:T(8,128)(2,1)S(1)}, u32[]{:S(2)}, u32[]{:S(2)}) async-start(bf16[32,16,2048]{2,1,0:T(8,128)(2,1)} %bitcast.48), calls=%async_computation.2 | async-start | bytes 4194304 | tf_op jit(solution)/shard_map/all_to_all | solution.py:84
where the time goes:
time: 164 us; the launch traced here: 163 us
  waiting for transfers between devices  54.5 us (33%)
  blocking collectives  52.4 us (32%)
  starting transfers between devices  15.6 us (10%)
  matrix products  15.3 us (9%)
  local copies, waits for them, and re-layouts  14.8 us (9%)
  other arithmetic  10.3 us (6%)
    all_to_all x1, blocking collectives, on_device(): lax.all_to_all(outgoing.reshape(experts_total, capacity, model_width), ('...  52.4 us
    all_to_all x1, waiting for transfers between devices, on_device(): lax.all_to_all(result, ('sp', 'tp'), split_axis=0, concat_axis=0, tiled=T...  48.5 us
    dot_general x1, matrix products, expert_rows(): jnp.dot(hidden, down_weight, preferred_element_type=jnp.float32)  9.94 us
    ppermute x2, starting transfers between devices, from_behind(): return lax.ppermute(block, axis, route)  8.32 us
    all_to_all x1, waiting for transfers between devices, on_device(): lax.all_to_all(conv_out, 'tp', split_axis=0, concat_axis=1, tiled=True)  5.96 us
    all_to_all x1, starting transfers between devices, on_device(): lax.all_to_all(result, ('sp', 'tp'), split_axis=0, concat_axis=0, tiled=T...  3.84 us
    scatter x1, local copies, waits for them, and re-layouts, on_device(): jnp.zeros((experts_total * capacity, model_width), jnp.bfloat16).at[target]  3.5 us
    all_to_all x1, starting transfers between devices, on_device(): lax.all_to_all(conv_out, 'tp', split_axis=0, concat_axis=1, tiled=True)  3.41 us
  transfers between devices with their start and end apart: 4, of which 2 were waited for; matrix products, arithmetic and copies ran while one was open for 4% of the time, Pallas kernels for 0%

commit v1 on v0

--- a/solution.py
+++ b/solution.py
@@ -1,7 +1,243 @@
+import functools
+
 import jax
 import jax.numpy as jnp
 from jax import lax
+from jax.experimental import pallas as pl
+from jax.experimental.pallas import tpu as pltpu
 from jax.sharding import PartitionSpec as P
+
+MESH = pl.DeviceIdType.MESH
+
+
+def layer_kernel(
+    sp_count, tp_count, cap, pieces,
+    x_ref, meta_ref, carried_ref, gate_hbm, up_hbm, down_hbm,
+    out_ref,
+    gate_w, up_w, down_w, meta_far, x_far, slots, arrived, hidden, served, back, part_out, part_in,
+    w_sem, meta_sem, dense_send, dense_recv, part_send, part_recv, go_send, go_recv, ret_send, ret_recv,
+):
+    sp = lax.axis_index("sp")
+    tp = lax.axis_index("tp")
+    half = sp_count // 2
+    group = half * tp_count
+    base = lax.div(sp, half) * half
+    mine = (sp - base) * tp_count + tp
+    far = (lax.rem(sp + half, sp_count), tp)
+    rows, width = x_ref.shape
+    step = width // pieces
+    ff = gate_w.shape[1]
+    tile = 256
+    slot_count = group * cap
+
+    def where(member):
+        return (base + lax.div(member, tp_count), lax.rem(member, tp_count))
+
+    def peer(i):
+        odd = lax.rem(i, 2)
+        shift = group // 2 + (1 - 2 * odd) * lax.div(i + 1, 2)
+        return lax.rem(mine + shift, group)
+
+    loads = [
+        pltpu.make_async_copy(source.at[0], target, w_sem.at[n])
+        for n, (source, target) in enumerate(((gate_hbm, gate_w), (up_hbm, up_w), (down_hbm, down_w)))
+    ]
+    for load in loads:
+        load.start()
+
+    barrier = pltpu.get_barrier_semaphore()
+    pl.semaphore_signal(barrier, inc=1, device_id=far, device_id_type=MESH)
+
+    @pl.loop(0, group - 1)
+    def _(i):
+        pl.semaphore_signal(barrier, inc=1, device_id=where(peer(i)), device_id_type=MESH)
+
+    pl.semaphore_wait(barrier, group)
+
+    def dense_copy(c):
+        return pltpu.make_async_remote_copy(
+            src_ref=x_ref.at[:, pl.ds(c * step, step)], dst_ref=x_far.at[c],
+            send_sem=dense_send.at[c], recv_sem=dense_recv.at[c], device_id=far, device_id_type=MESH,
+        )
+
+    def part_copy(c):
+        return pltpu.make_async_remote_copy(
+            src_ref=part_out.at[c], dst_ref=part_in.at[c],
+            send_sem=part_send.at[c], recv_sem=part_recv.at[c], device_id=far, device_id_type=MESH,
+        )
+
+    def exchange(source, target, send, recv, p, c, other, landing):
+        return pltpu.make_async_remote_copy(
+            src_ref=source.at[p, c, other], dst_ref=target.at[p, c, landing],
+            send_sem=send.at[p, c, other], recv_sem=recv.at[p, c, landing],
+            device_id=where(other), device_id_type=MESH,
+        )
+
+    def send_all(source, target, send, recv, p, c):
+        @pl.loop(0, group - 1)
+        def _(i):
+            exchange(source, target, send, recv, p, c, peer(i), mine).start()
+
+        target[p, c, pl.ds(mine, 1)] = source[p, c, pl.ds(mine, 1)]
+
+    def wait_all(source, target, send, recv, p, c):
+        @pl.loop(0, group - 1)
+        def _(i):
+            other = peer(i)
+            exchange(source, target, send, recv, p, c, other, other).wait_recv()
+
+    def wait_sent(source, target, send, recv):
+        for p in range(2):
+            @pl.loop(0, pieces)
+            def _(c):
+                @pl.loop(0, group - 1)
+                def _(i):
+                    other = peer(i)
+                    exchange(source, target, send, recv, p, c, other, other).wait_send()
+
+    go = (slots, arrived, go_send, go_recv)
+    ret = (served, back, ret_send, ret_recv)
+
+    meta_copy = pltpu.make_async_remote_copy(
+        src_ref=meta_ref, dst_ref=meta_far, send_sem=meta_sem.at[0], recv_sem=meta_sem.at[1],
+        device_id=far, device_id_type=MESH,
+    )
+    meta_copy.start()
+
+    def matches(meta):
+        first = base * tp_count * cap
+        ids = (lax.broadcasted_iota(jnp.int32, (slot_count, rows), 0) + first).astype(jnp.float32)
+        choices = meta.shape[0] // 2
+        return [(meta[k : k + 1, :] == ids, meta[choices + k : choices + k + 1, :]) for k in range(choices)]
+
+    def placing(meta):
+        total = jnp.zeros((slot_count, rows), jnp.float32)
+        for hit, _ in matches(meta):
+            total = total + jnp.where(hit, 1.0, 0.0)
+        return total.astype(jnp.bfloat16)
+
+    def weighing(meta):
+        total = jnp.zeros((slot_count, rows), jnp.float32)
+        for hit, weight in matches(meta):
+            total = total + jnp.where(hit, weight, 0.0)
+        total = total.T
+        high = total.astype(jnp.bfloat16)
+        return high, (total - high.astype(jnp.float32)).astype(jnp.bfloat16)
+
+    def fill(p, c, place, block):
+        picked = jnp.dot(place, block, preferred_element_type=jnp.float32).astype(jnp.bfloat16)
+        slots[p, c] = picked.reshape(group, cap, step)
+        send_all(*go, p, c)
+
+    place = placing(meta_ref[...])
+    for c in range(pieces):
+        dense_copy(c).start()
+        fill(0, c, place, x_ref[:, c * step : (c + 1) * step])
+
+    meta_copy.wait()
+    place = placing(meta_far[...])
+    for c in range(pieces):
+        dense_copy(c).wait_recv()
+        fill(1, c, place, x_far[c])
+
+    for p in range(2):
+        for c in range(pieces):
+            wait_all(*go, p, c)
+        if p == 0:
+            loads[0].wait()
+            loads[1].wait()
+
+        @pl.loop(0, ff // tile)
+        def _(f):
+            columns = pl.ds(pl.multiple_of(f * tile, tile), tile)
+            gate_value = jnp.zeros((slot_count, tile), jnp.float32)
+            up_value = jnp.zeros((slot_count, tile), jnp.float32)
+            for c in range(pieces):
+                piece = arrived[p, c].reshape(slot_count, step)
+                lines = pl.ds(c * step, step)
+                gate_value += jnp.dot(piece, gate_w[lines, columns], preferred_element_type=jnp.float32)
+                up_value += jnp.dot(piece, up_w[lines, columns], preferred_element_type=jnp.float32)
+            silu = gate_value * (1.0 / (1.0 + jnp.exp(-gate_value)))
+            hidden[:, columns] = (silu * up_value).astype(jnp.bfloat16)
+
+        if p == 0:
+            loads[2].wait()
+
+        for c in range(pieces):
+            value = jnp.dot(
+                hidden[...], down_w[:, c * step : (c + 1) * step], preferred_element_type=jnp.float32
+            ).astype(jnp.bfloat16)
+            served[p, c] = value.reshape(group, cap, step)
+            send_all(*ret, p, c)
+
+    def weighted(p, c, high, low):
+        got = back[p, c].reshape(slot_count, step)
+        return jnp.dot(high, got, preferred_element_type=jnp.float32) + jnp.dot(
+            low, got, preferred_element_type=jnp.float32
+        )
+
+    high, low = weighing(meta_far[...])
+    for c in range(pieces):
+        wait_all(*ret, 1, c)
+        part_out[c] = weighted(1, c, high, low).astype(jnp.bfloat16)
+        part_copy(c).start()
+    high, low = weighing(meta_ref[...])
+    for c in range(pieces):
+        wait_all(*ret, 0, c)
+        total = carried_ref[:, c * step : (c + 1) * step] + weighted(0, c, high, low)
+        part_copy(c).wait_recv()
+        out_ref[:, c * step : (c + 1) * step] = (total + part_in[c].astype(jnp.float32)).astype(jnp.bfloat16)
+
+    for c in range(pieces):
+        dense_copy(c).wait_send()
+        part_copy(c).wait_send()
+    wait_sent(*go)
+    wait_sent(*ret)
+
+
+def run_layer(normed, meta, carried, gate_proj, up_proj, down_proj, cap, pieces=4):
+    sp_count, tp_count = lax.axis_size("sp"), lax.axis_size("tp")
+    rows, width = normed.shape
+    ff = gate_proj.shape[2]
+    group = sp_count // 2 * tp_count
+    step = width // pieces
+    slot_shape = (2, pieces, group, cap, step)
+    dma = pltpu.SemaphoreType.DMA
+    vmem = pl.BlockSpec(memory_space=pltpu.VMEM)
+    hbm = pl.BlockSpec(memory_space=pl.ANY)
+    return pl.pallas_call(
+        functools.partial(layer_kernel, sp_count, tp_count, cap, pieces),
+        out_shape=jax.ShapeDtypeStruct((rows, width), jnp.bfloat16),
+        in_specs=[vmem, vmem, vmem, hbm, hbm, hbm],
+        out_specs=vmem,
+        scratch_shapes=[
+            pltpu.VMEM((width, ff), jnp.bfloat16),
+            pltpu.VMEM((width, ff), jnp.bfloat16),
+            pltpu.VMEM((ff, width), jnp.bfloat16),
+            pltpu.VMEM(meta.shape, jnp.float32),
+            pltpu.VMEM((pieces, rows, step), jnp.bfloat16),
+            pltpu.VMEM(slot_shape, jnp.bfloat16),
+            pltpu.VMEM(slot_shape, jnp.bfloat16),
+            pltpu.VMEM((group * cap, ff), jnp.bfloat16),
+            pltpu.VMEM(slot_shape, jnp.bfloat16),
+            pltpu.VMEM(slot_shape, jnp.bfloat16),
+            pltpu.VMEM((pieces, rows, step), jnp.bfloat16),
+            pltpu.VMEM((pieces, rows, step), jnp.bfloat16),
+            dma((3,)),
+            dma((2,)),
+            dma((pieces,)),
+            dma((pieces,)),
+            dma((pieces,)),
+            dma((pieces,)),
+            dma((2, pieces, group)),
+            dma((2, pieces, group)),
+            dma((2, pieces, group)),
+            dma((2, pieces, group)),
+        ],
+        compiler_params=pltpu.CompilerParams(
+            collective_id=0, has_side_effects=True, vmem_limit_bytes=48 * 1024 * 1024
+        ),
+    )(normed, meta, carried, gate_proj, up_proj, down_proj)
 
 
 def from_behind(block, axis, distance):
@@ -63,6 +299,10 @@
     )
     slot_rank = jnp.sum((jnp.cumsum(onehot, axis=0) - 1) * onehot, axis=1)
     target = flat_ids * capacity + slot_rank
+    if capacity % 16 == 0 and sp_count % 2 == 0:
+        places = target.reshape(row_count, choose).astype(jnp.float32)
+        meta = jnp.concatenate([places.T, expert_weights.T], axis=0)
+        return run_layer(normed, meta, carried, gate_proj, up_proj, down_proj, capacity)
     sources = jnp.repeat(normed, choose, axis=0)
     outgoing = (
         jnp.zeros((experts_total * capacity, model_width), jnp.bfloat16).at[target].set(sources)

time: 164 us -> 119 us (0.73)
  Pallas kernels: 0 us -> 88 us
  blocking collectives: 52.4 us -> 0 us
  waiting for transfers between devices: 54.5 us -> 4.6 us
  matrix products: 15.3 us -> 3.13 us
  local copies, waits for them, and re-layouts: 14.8 us -> 3.99 us
  starting transfers between devices: 15.6 us -> 11.7 us
  other arithmetic: 10.3 us -> 6.83 us
    pallas_call x0 -> x1, Pallas kernels: none -> 88 us  [run_layer(): pl.pallas_call(functools.partial(layer_kernel, sp_count, tp_count, cap, p...]
    all_to_all x1 -> x0, blocking collectives: 52.4 us -> none  [on_device(): lax.all_to_all(outgoing.reshape(experts_total, capacity, model_width), ('...]
    all_to_all x1 -> x0, waiting for transfers between devices: 48.5 us -> none  [on_device(): lax.all_to_all(result, ('sp', 'tp'), split_axis=0, concat_axis=0, tiled=T...]
    dot_general x2 -> x0, matrix products: 12.3 us -> none  [the longest x1 9.94 us: expert_rows(): jnp.dot(hidden, down_weight, preferred_element_type=jnp.float32)]
    all_to_all x1 -> x0, starting transfers between devices: 3.84 us -> none  [on_device(): lax.all_to_all(result, ('sp', 'tp'), split_axis=0, concat_axis=0, tiled=T...]
    scatter x1 -> x0, local copies, waits for them, and re-layouts: 3.5 us -> none  [on_device(): jnp.zeros((experts_total * capacity, model_width), jnp.bfloat16).at[target]]
    reduce_sum x1 -> x0, other arithmetic: 3.16 us -> none  [on_device(): combined = carried + jnp.sum(expert_weights[:, :, None] * picked, axis=1)]
    convert_element_type x1 -> x0, local copies, waits for them, and re-layouts: 2.37 us -> none  [on_device(): picked = returned.reshape(-1, model_width)[target].reshape(row_count, cho...]
  transfers between devices with their start and end apart: 4 -> 3, of which waited for: 2 -> 1; matrix products, arithmetic and copies ran while one was open for 4% -> 6% of each run, Pallas kernels for 0% -> 0%
where the time goes in v1:
time: 119 us; the launch traced here: 118 us
  Pallas kernels  88 us (74%)
  starting transfers between devices  11.7 us (10%)
  other arithmetic  6.83 us (6%)
  waiting for transfers between devices  4.6 us (4%)
  local copies, waits for them, and re-layouts  3.99 us (3%)
  matrix products  3.13 us (3%)
    pallas_call x1, Pallas kernels, run_layer(): pl.pallas_call(functools.partial(layer_kernel, sp_count, tp_count, cap, p...  88 us
    ppermute x2, starting transfers between devices, from_behind(): return lax.ppermute(block, axis, route)  8.32 us
    all_to_all x1, waiting for transfers between devices, on_device(): lax.all_to_all(conv_out, 'tp', split_axis=0, concat_axis=1, tiled=True)  4.6 us
    all_to_all x1, starting transfers between devices, on_device(): lax.all_to_all(conv_out, 'tp', split_axis=0, concat_axis=1, tiled=True)  3.41 us
    dot_general x1, matrix products, on_device(): jnp.dot(regrouped, out_proj, preferred_element_type=jnp.float32)  3.13 us
  transfers between devices with their start and end apart: 3, of which 1 were waited for; matrix products, arithmetic and copies ran while one was open for 6% of the time, Pallas kernels for 0%

profile of v1, /device:TPU:0, one launch (start us, length us, event | category | flops | bytes accessed | tf_op | source)
XLA Modules:
  0.0 118.3 jit_solution(9316395767740413492)
XLA Ops:
  0.0 0.8 slice.35
  0.8 4.9 %collective-permute-start = (s32[2]{0:T(128)S(1)}, s32[2]{0:T(128)S(1)}, u32[]{:S(2)}, u32[]{:S(2)}) collective-permute-start(s32[2]{0:T(128)S(1)} %slice.35), channel_id=1, source_target_pairs={{0,4},{4,8},{8,12},{12,16},{16,20},{20,24},{24,28},{1,5},{5,9},{9,... | collective-permute-start | bytes 32 | tf_op jit(solution)/shard_map/ppermute | solution.py:246
  5.6 1.1 convert_multiply_fusion
  6.8 3.4 %collective-permute-start.1 = (f32[2,256]{1,0:T(2,128)S(1)}, f32[2,256]{1,0:T(2,128)S(1)}, u32[]{:S(2)}, u32[]{:S(2)}) collective-permute-start(f32[2,256]{1,0:T(2,128)S(1)} %slice.46), channel_id=1, source_target_pairs={{0,4},{4,8},{8,12},{12,16},{16,20},{20,24},{24,28},{1,5},{5,9},{9,... | collective-permute-start | bytes 6152 | tf_op jit(solution)/shard_map/ppermute | solution.py:246
  10.2 0.8 copy.19
  11.0 0.1 eq.37
  11.1 0.1 eq.33
  11.3 0.8 fusion.14
  12.1 0.6 reduce-window.6
  12.7 0.2 slice_reduce_fusion
  12.9 0.1 fusion.12
  13.0 0.1 reduce_sum.22
  13.2 0.8 pad_add_fusion
  14.0 0.8 slice_compare_fusion.1
  14.7 1.9 %fusion.8 = bf16[512,256]{1,0:T(8,128)(2,1)} fusion(f32[2,256]{1,0:T(2,128)S(1)} %collective-permute-done.1, f32[512,256]{1,0:T(8,128)S(1)} %convert_multiply_fusion, bf16[512,256]{1,0:T(8,128)(2,1)} %param.15, f32[256]{0:T(256)S(1)} %bitcast.30, f32[256]{0:T(256)S(1)} %bitcast.29, f32[256]{0:T(256)S(1)} %bitcast.28, pred[512]{0:T(512)(128)(4,1)S(1)} %get-tuple-element.6, ...), kind=kLoop, calls=%fused_computation.13 | loop fusion | flops 1572864 | bytes 1054720 | tf_op jit(solution)/shard_map/convert_element_type | solution.py:282
  16.7 3.4 %all-to-all-start = ((bf16[4,128,256]{2,1,0:T(8,128)(2,1)}), bf16[4,128,256]{2,1,0:T(8,128)(2,1)S(1)}, u32[]{:S(2)}, u32[]{:S(2)}) async-start(bf16[4,128,256]{2,1,0:T(8,128)(2,1)} %bitcast.3), calls=%async_computation | async-start | bytes 524288 | tf_op jit(solution)/shard_map/all_to_all | solution.py:284
  20.1 0.7 convert_bitcast_fusion
  20.8 0.7 pad_maximum_fusion.1.meta_ref
  21.5 4.6 %all-to-all-done = bf16[4,128,256]{2,1,0:T(8,128)(2,1)S(1)} async-done(((bf16[4,128,256]{2,1,0:T(8,128)(2,1)}), bf16[4,128,256]{2,1,0:T(8,128)(2,1)S(1)}, u32[]{:S(2)}, u32[]{:S(2)}) %all-to-all-start) | async-done | bytes 262176 | tf_op jit(solution)/shard_map/all_to_all | solution.py:284
  26.1 0.2 copy.18
  26.3 3.1 %multiply_reduce_fusion = (f32[128]{0:T(128)S(1)}, f32[128,2048]{1,0:T(8,128)S(1)}) fusion(bf16[128,1024]{0,1:T(8,128)(2,1)S(1)} %bitcast.26, bf16[1024,2048]{1,0:T(8,128)(2,1)} %param.19, bf16[128,2048]{1,0:T(8,128)(2,1)} %param.18), kind=kOutput, calls=%fused_computation.4 | convolution fusion | flops 538443648 | bytes 6029824 | tf_op jit(solution)/shard_map/dot_general | solution.py:285
  29.4 0.2 multiply_convert_fusion.x_ref
  29.6 88.0 %shard_map.127 = bf16[128,2048]{1,0:T(8,128)(2,1)S(1)} custom-call(bf16[128,2048]{1,0:T(8,128)(2,1)S(1)} %multiply_convert_fusion.x_ref, f32[4,128]{1,0:T(4,128)S(1)} %pad_maximum_fusion.1.meta_ref, f32[128,2048]{1,0:T(8,128)S(1)} %get-tuple-element.11.carried_ref, bf16[1,2048,1024]{2,1,0:T(8,128)(2,1)} %gate_hbm.1, bf16[1,2048,1024]{2,1,0:T(8,128)(2,1)} %up_hbm.1, ...), custom_call_target="tpu_custom_call" | custom-call | tf_op jit(solution)/shard_map/pallas_call | solution.py:208
  117.5 0.8 copy.26
  (10 shorter events, 0.1 us)
Async XLA Ops:
  0.8 12.5 %collective-permute-start = (s32[2]{0:T(128)S(1)}, s32[2]{0:T(128)S(1)}, u32[]{:S(2)}, u32[]{:S(2)}) collective-permute-start(s32[2]{0:T(128)S(1)} %slice.35), channel_id=1, source_target_pairs={{0,4},{4,8},{8,12},{12,16},{16,20},{20,24},{24,28},{1,5},{5,9},{9,... | collective-permute-start | bytes 32 | tf_op jit(solution)/shard_map/ppermute | solution.py:246
  6.8 8.0 %collective-permute-start.1 = (f32[2,256]{1,0:T(2,128)S(1)}, f32[2,256]{1,0:T(2,128)S(1)}, u32[]{:S(2)}, u32[]{:S(2)}) collective-permute-start(f32[2,256]{1,0:T(2,128)S(1)} %slice.46), channel_id=1, source_target_pairs={{0,4},{4,8},{8,12},{12,16},{16,20},{20,24},{24,28},{1,5},{5,9},{9,... | collective-permute-start | bytes 6152 | tf_op jit(solution)/shard_map/ppermute | solution.py:246
  12.7 16.7 %copy-start = (f32[2048]{0:T(1024)S(1)}, f32[2048]{0:T(1024)}, u32[]{:S(2)}) copy-start(f32[2048]{0:T(1024)} %param.20) | copy-start | bytes 24580
  16.7 9.4 %all-to-all-start = ((bf16[4,128,256]{2,1,0:T(8,128)(2,1)}), bf16[4,128,256]{2,1,0:T(8,128)(2,1)S(1)}, u32[]{:S(2)}, u32[]{:S(2)}) async-start(bf16[4,128,256]{2,1,0:T(8,128)(2,1)} %bitcast.3), calls=%async_computation | async-start | bytes 524288 | tf_op jit(solution)/shard_map/all_to_all | solution.py:284

commit v2 on v1

--- a/solution.py
+++ b/solution.py
@@ -12,10 +12,12 @@
 
 def layer_kernel(
     sp_count, tp_count, cap, pieces,
-    x_ref, meta_ref, carried_ref, gate_hbm, up_hbm, down_hbm,
+    conv_ref, inner_ref, outer_ref, taps_ref, docs_ref, residual_ref, gain_ref,
+    meta_ref, gate_hbm, up_hbm, down_hbm, proj_hbm,
     out_ref,
+    x_ref, carried_ref, proj_w, padded, padded_docs, tail, tail_in, conv_out, conv_in,
     gate_w, up_w, down_w, meta_far, x_far, slots, arrived, hidden, served, back, part_out, part_in,
-    w_sem, meta_sem, dense_send, dense_recv, part_send, part_recv, go_send, go_recv, ret_send, ret_recv,
+    w_sem, tail_sem, conv_send, conv_recv, meta_sem, dense_send, dense_recv, part_send, part_recv, go_send, go_recv, ret_send, ret_recv,
 ):
     sp = lax.axis_index("sp")
     tp = lax.axis_index("tp")
@@ -38,11 +40,12 @@
         shift = group // 2 + (1 - 2 * odd) * lax.div(i + 1, 2)
         return lax.rem(mine + shift, group)
 
+    pairs = ((gate_hbm.at[0], gate_w), (up_hbm.at[0], up_w), (down_hbm.at[0], down_w), (proj_hbm, proj_w))
     loads = [
-        pltpu.make_async_copy(source.at[0], target, w_sem.at[n])
-        for n, (source, target) in enumerate(((gate_hbm, gate_w), (up_hbm, up_w), (down_hbm, down_w)))
+        pltpu.make_async_copy(source, target, w_sem.at[n])
+        for n, (source, target) in enumerate(pairs)
     ]
-    for load in loads:
+    for load in loads[3:] + loads[:3]:
         load.start()
 
     barrier = pltpu.get_barrier_semaphore()
@@ -52,7 +55,64 @@
     def _(i):
         pl.semaphore_signal(barrier, inc=1, device_id=where(peer(i)), device_id_type=MESH)
 
-    pl.semaphore_wait(barrier, group)
+    after = (lax.rem(sp + 1, sp_count), tp)
+    before = (lax.rem(sp + sp_count - 1, sp_count), tp)
+    for neighbour in (after, before):
+        pl.semaphore_signal(barrier, inc=1, device_id=neighbour, device_id_type=MESH)
+
+    length, channels = conv_ref.shape
+    lanes = docs_ref.shape[1]
+    edge = tail.shape[0]
+    padded[edge:, :] = conv_ref[...].astype(jnp.float32) * inner_ref[...].astype(jnp.float32)
+    padded_docs[edge:, :] = docs_ref[...]
+    tail[:, :channels] = padded[length:, :]
+    tail[:, channels:] = padded_docs[length:, :]
+    pl.semaphore_wait(barrier, group + 2)
+
+    tail_copy = pltpu.make_async_remote_copy(
+        src_ref=tail, dst_ref=tail_in, send_sem=tail_sem.at[0], recv_sem=tail_sem.at[1],
+        device_id=after, device_id_type=MESH,
+    )
+    tail_copy.start()
+    tail_copy.wait()
+    padded[:edge, :] = tail_in[:, :channels]
+    padded_docs[:edge, :] = jnp.where(sp == 0, -1.0, tail_in[:, channels:])
+    docs = docs_ref[...]
+    same_one = padded_docs[edge - 1 : edge - 1 + length, :] == docs
+    same_two = padded_docs[edge - 2 : edge - 2 + length, :] == docs
+    taps = taps_ref[...].astype(jnp.float32)
+    for k in range(channels // lanes):
+        at = slice(k * lanes, (k + 1) * lanes)
+        one_back = jnp.where(same_one, padded[edge - 1 : edge - 1 + length, at], 0.0)
+        two_back = jnp.where(same_two, padded[edge - 2 : edge - 2 + length, at], 0.0)
+        mixed = taps[2:3, at] * padded[edge:, at] + taps[1:2, at] * one_back + taps[0:1, at] * two_back
+        gated = (outer_ref[:, at].astype(jnp.float32) * mixed).astype(jnp.bfloat16)
+        conv_out[:, :, at] = gated.reshape(tp_count, rows, lanes)
+
+    def conv_copy(other, landing):
+        return pltpu.make_async_remote_copy(
+            src_ref=conv_out.at[other], dst_ref=conv_in.at[landing],
+            send_sem=conv_send.at[other], recv_sem=conv_recv.at[landing],
+            device_id=(sp, other), device_id_type=MESH,
+        )
+
+    others = [lax.rem(tp + j, tp_count) for j in range(1, tp_count)]
+    for other in others:
+        conv_copy(other, tp).start()
+    conv_in[pl.ds(tp, 1)] = conv_out[pl.ds(tp, 1)]
+    loads[3].wait()
+    for other in others:
+        conv_copy(other, other).wait_recv()
+    for c in range(pieces):
+        at = slice(c * step, (c + 1) * step)
+        mix = jnp.zeros((rows, step), jnp.float32)
+        for j in range(tp_count):
+            lines = slice(j * channels, (j + 1) * channels)
+            mix += jnp.dot(conv_in[j], proj_w[lines, at], preferred_element_type=jnp.float32)
+        carried_ref[:, at] = residual_ref[:, at].astype(jnp.float32) + mix.astype(jnp.bfloat16).astype(jnp.float32)
+    carried = carried_ref[...]
+    scale = lax.rsqrt(jnp.mean(carried * carried, axis=1, keepdims=True) + 1e-06)
+    x_ref[...] = (carried * scale * gain_ref[...]).astype(jnp.bfloat16)
 
     def dense_copy(c):
         return pltpu.make_async_remote_copy(
@@ -188,6 +248,8 @@
         part_copy(c).wait_recv()
         out_ref[:, c * step : (c + 1) * step] = (total + part_in[c].astype(jnp.float32)).astype(jnp.bfloat16)
 
+    for other in others:
+        conv_copy(other, other).wait_send()
     for c in range(pieces):
         dense_copy(c).wait_send()
         part_copy(c).wait_send()
@@ -195,9 +257,12 @@
     wait_sent(*ret)
 
 
-def run_layer(normed, meta, carried, gate_proj, up_proj, down_proj, cap, pieces=4):
+def run_layer(front, meta, gate_proj, up_proj, down_proj, out_proj, cap, pieces=4):
     sp_count, tp_count = lax.axis_size("sp"), lax.axis_size("tp")
-    rows, width = normed.shape
+    length, channels = front[0].shape
+    lanes = front[4].shape[1]
+    rows, width = front[5].shape
+    edge = 8
     ff = gate_proj.shape[2]
     group = sp_count // 2 * tp_count
     step = width // pieces
@@ -208,9 +273,18 @@
     return pl.pallas_call(
         functools.partial(layer_kernel, sp_count, tp_count, cap, pieces),
         out_shape=jax.ShapeDtypeStruct((rows, width), jnp.bfloat16),
-        in_specs=[vmem, vmem, vmem, hbm, hbm, hbm],
+        in_specs=[vmem] * 8 + [hbm] * 4,
         out_specs=vmem,
         scratch_shapes=[
+            pltpu.VMEM((rows, width), jnp.bfloat16),
+            pltpu.VMEM((rows, width), jnp.float32),
+            pltpu.VMEM(out_proj.shape, jnp.bfloat16),
+            pltpu.VMEM((edge + length, channels), jnp.float32),
+            pltpu.VMEM((edge + length, lanes), jnp.float32),
+            pltpu.VMEM((edge, channels + lanes), jnp.float32),
+            pltpu.VMEM((edge, channels + lanes), jnp.float32),
+            pltpu.VMEM((tp_count, rows, channels), jnp.bfloat16),
+            pltpu.VMEM((tp_count, rows, channels), jnp.bfloat16),
             pltpu.VMEM((width, ff), jnp.bfloat16),
             pltpu.VMEM((width, ff), jnp.bfloat16),
             pltpu.VMEM((ff, width), jnp.bfloat16),
@@ -223,7 +297,10 @@
             pltpu.VMEM(slot_shape, jnp.bfloat16),
             pltpu.VMEM((pieces, rows, step), jnp.bfloat16),
             pltpu.VMEM((pieces, rows, step), jnp.bfloat16),
-            dma((3,)),
+            dma((4,)),
+            dma((2,)),
+            dma((tp_count,)),
+            dma((tp_count,)),
             dma((2,)),
             dma((pieces,)),
             dma((pieces,)),
@@ -237,7 +314,7 @@
         compiler_params=pltpu.CompilerParams(
             collective_id=0, has_side_effects=True, vmem_limit_bytes=48 * 1024 * 1024
         ),
-    )(normed, meta, carried, gate_proj, up_proj, down_proj)
+    )(*front, meta, gate_proj, up_proj, down_proj, out_proj)
 
 
 def from_behind(block, axis, distance):
@@ -302,7 +379,9 @@
     if capacity % 16 == 0 and sp_count % 2 == 0:
         places = target.reshape(row_count, choose).astype(jnp.float32)
         meta = jnp.concatenate([places.T, expert_weights.T], axis=0)
-        return run_layer(normed, meta, carried, gate_proj, up_proj, down_proj, capacity)
+        docs = jnp.broadcast_to(doc_ids.astype(jnp.float32)[:, None], (doc_ids.shape[0], 128))
+        front = (conv_input, gate_inner, gate_outer, conv_taps, docs, residual_in, norm_gain[None, :])
+        return run_layer(front, meta, gate_proj, up_proj, down_proj, out_proj, capacity)
     sources = jnp.repeat(normed, choose, axis=0)
     outgoing = (
         jnp.zeros((experts_total * capacity, model_width), jnp.bfloat16).at[target].set(sources)

time: 119 us -> 109 us (0.916)
  starting transfers between devices: 11.7 us -> 0 us
  Pallas kernels: 88 us -> 98.1 us
  waiting for transfers between devices: 4.6 us -> 0 us
  other arithmetic: 6.83 us -> 2.81 us
  local copies, waits for them, and re-layouts: 3.99 us -> 7.63 us
  matrix products: 3.13 us -> 0 us
    pallas_call x1, Pallas kernels: 88 us -> 98.1 us  [run_layer(): pl.pallas_call(functools.partial(layer_kernel, sp_count, tp_count, cap, p...]
    ppermute x2 -> x0, starting transfers between devices: 8.32 us -> none  [from_behind(): return lax.ppermute(block, axis, route)]
    unnamed x4 -> x14, local copies, waits for them, and re-layouts: 1.59 us -> 6.85 us
    all_to_all x1 -> x0, waiting for transfers between devices: 4.6 us -> none  [on_device(): lax.all_to_all(conv_out, 'tp', split_axis=0, concat_axis=1, tiled=True)]
    all_to_all x1 -> x0, starting transfers between devices: 3.41 us -> none  [on_device(): lax.all_to_all(conv_out, 'tp', split_axis=0, concat_axis=1, tiled=True)]
    dot_general x1 -> x0, matrix products: 3.13 us -> none  [on_device(): jnp.dot(regrouped, out_proj, preferred_element_type=jnp.float32)]
    slice x4 -> x1, local copies, waits for them, and re-layouts: 1.74 us -> 0.18 us  [the longest x1 0.8 us: on_device(): tap_values[2] * inner_prod + tap_values[1] * one_back]
    convert_element_type x2 -> x1, other arithmetic: 2.1 us -> 0.68 us  [on_device(): doc_ids.astype(jnp.float32)[:, None]]
  transfers between devices with their start and end apart: 3 -> 0, of which waited for: 1 -> 0; matrix products, arithmetic and copies ran while one was open for 6% -> 0% of each run, Pallas kernels for 0% -> 0%
where the time goes in v2:
time: 109 us
  Pallas kernels  98.1 us (90%)
  local copies, waits for them, and re-layouts  7.63 us (7%)
  other arithmetic  2.81 us (3%)
    pallas_call x1, Pallas kernels, run_layer(): pl.pallas_call(functools.partial(layer_kernel, sp_count, tp_count, cap, p...  98.1 us
    unnamed x14, local copies, waits for them, and re-layouts  6.85 us

profile of v2, /device:TPU:0, one launch (start us, length us, event | category | flops | bytes accessed | tf_op | source)
XLA Modules:
  0.0 108.6 jit_solution(13044616005017743196)
XLA Ops:
  0.0 0.7 convert_element_type.11
  0.7 0.8 copy.14
  1.5 0.1 eq.29
  1.6 0.1 eq.25
  1.8 0.6 reduce-window.6
  2.4 0.2 slice_reduce_fusion
  2.6 0.1 fusion.1
  2.7 0.1 reduce_sum.12
  2.8 0.1 copy.17
  2.9 0.7 convert_bitcast_fusion
  3.6 0.7 pad_maximum_fusion.meta_ref
  4.3 0.1 broadcast_in_dim.4.docs_ref
  4.4 0.0 copy-start
  4.4 1.0 copy-done
  5.5 0.0 copy-start.1
  5.5 0.9 copy-done.1
  6.4 0.9 copy-done.2
  7.4 0.0 copy-start.3
  7.4 0.9 copy-done.3
  8.3 0.0 copy-start.4
  8.3 0.7 copy-done.4
  9.0 0.7 copy-done.5
  9.7 98.1 %shard_map.127 = bf16[128,2048]{1,0:T(8,128)(2,1)S(1)} custom-call(bf16[512,256]{1,0:T(8,128)(2,1)S(1)} %copy-done.1, bf16[512,256]{1,0:T(8,128)(2,1)S(1)} %copy-done.2, bf16[512,256]{1,0:T(8,128)(2,1)S(1)} %copy-done.3, bf16[3,256]{1,0:T(4,128)(2,1)S(1)} %copy-done.5, f32[512,128]{1,0:T(8,128)S(1)} %broadcast_in_dim.4.docs_ref, ...), custom_call_target="tpu_custom_call" | custom-call | tf_op jit(solution)/shard_map/pallas_call | solution.py:273
  107.8 0.8 copy.21
  (5 shorter events, 0.1 us)
Async XLA Ops:
  4.4 1.0 copy-start
  5.5 0.9 copy-start.1
  6.4 0.9 copy-start.2
  7.4 0.9 copy-start.3
  8.3 0.7 copy-start.4
  9.0 0.7 copy-start.5

commit v3 on v2

--- a/solution.py
+++ b/solution.py
@@ -257,7 +257,7 @@
     wait_sent(*ret)
 
 
-def run_layer(front, meta, gate_proj, up_proj, down_proj, out_proj, cap, pieces=4):
+def run_layer(front, meta, gate_proj, up_proj, down_proj, out_proj, cap, pieces=2):
     sp_count, tp_count = lax.axis_size("sp"), lax.axis_size("tp")
     length, channels = front[0].shape
     lanes = front[4].shape[1]

time: 109 us -> 108 us (level)
  no operation moved by 1% of the time
where the time goes in v3:
time: 108 us
  Pallas kernels  97.1 us (90%)
  local copies, waits for them, and re-layouts  7.63 us (7%)
  other arithmetic  2.81 us (3%)
    pallas_call x1, Pallas kernels, run_layer(): pl.pallas_call(functools.partial(layer_kernel, sp_count, tp_count, cap, p...  97.1 us
    unnamed x14, local copies, waits for them, and re-layouts  6.85 us

profile of v3, /device:TPU:0, one launch (start us, length us, event | category | flops | bytes accessed | tf_op | source)
XLA Modules:
  0.0 107.6 jit_solution(18279076037329368788)
XLA Ops:
  0.0 0.7 convert_element_type.11
  0.7 0.8 copy.14
  1.5 0.1 eq.29
  1.6 0.1 eq.25
  1.8 0.6 reduce-window.6
  2.4 0.2 slice_reduce_fusion
  2.6 0.1 fusion.1
  2.7 0.1 reduce_sum.12
  2.8 0.1 copy.17
  2.9 0.7 convert_bitcast_fusion
  3.6 0.7 pad_maximum_fusion.meta_ref
  4.3 0.1 broadcast_in_dim.4.docs_ref
  4.4 0.0 copy-start
  4.4 1.0 copy-done
  5.5 0.0 copy-start.1
  5.5 0.9 copy-done.1
  6.4 0.9 copy-done.2
  7.4 0.0 copy-start.3
  7.4 0.9 copy-done.3
  8.3 0.0 copy-start.4
  8.3 0.7 copy-done.4
  9.0 0.7 copy-done.5
  9.7 97.1 %shard_map.127 = bf16[128,2048]{1,0:T(8,128)(2,1)S(1)} custom-call(bf16[512,256]{1,0:T(8,128)(2,1)S(1)} %copy-done.1, bf16[512,256]{1,0:T(8,128)(2,1)S(1)} %copy-done.2, bf16[512,256]{1,0:T(8,128)(2,1)S(1)} %copy-done.3, bf16[3,256]{1,0:T(4,128)(2,1)S(1)} %copy-done.5, f32[512,128]{1,0:T(8,128)S(1)} %broadcast_in_dim.4.docs_ref, ...), custom_call_target="tpu_custom_call" | custom-call | tf_op jit(solution)/shard_map/pallas_call | solution.py:273
  106.8 0.8 copy.21
  (5 shorter events, 0.1 us)
Async XLA Ops:
  4.4 1.0 copy-start
  5.5 0.9 copy-start.1
  6.4 0.9 copy-start.2
  7.4 0.9 copy-start.3
  8.3 0.7 copy-start.4
  9.0 0.7 copy-start.5
